TPU v7x, 32 devices: a whole 2x2x4 slice. The times are simulated.
32 devices in a mesh: rep: 4 (over z), fs: 4 (over y, x), tp: 2 (over core).
Axes of the slice: x: 2, y: 2, z: 4, core: 2. Of those that a mesh axis runs over, the one named last changes fastest.
Arguments:
- inputs: bfloat16 [512, 2048], P(('rep', 'fs', 'tp')), may hold values from -6 to 6
- cotangent: bfloat16 [512, 2048], P(('rep', 'fs', 'tp')), may hold values from -6 to 6
- norm_gain: float32 [2048], replicated, may hold values from 0.1 to 1.9
- gate_weight: bfloat16 [2048, 2816], P(None, ('fs', 'tp')), may hold values from -0.125 to 0.125
- up_weight: bfloat16 [2048, 2816], P(None, ('fs', 'tp')), may hold values from -0.125 to 0.125
- down_weight: bfloat16 [2816, 2048], P(('fs', 'tp')), may hold values from -0.109375 to 0.109375
Outputs:
- input_grad: bfloat16 [512, 2048], P(('rep', 'fs', 'tp'))
- gain_grad: float32 [2048], replicated
- down_grad: float32 [2816, 2048], P(('fs', 'tp'), 'rep')
All inputs are finite; a program needn't handle non-finite values.
Results may differ from a plain program's by a relative error of at most 0.0066.
Values may be sent and summed in bfloat16 or wider, within the bound.
A program may use at most 64 MiB of HBM per device.

v0:
```python
import jax
import jax.numpy as jnp
from jax import lax
from jax.sharding import PartitionSpec as P

EPS = 1e-06


def across_tokens(left, right):
    return lax.dot_general(
        left, right, (((0,), (0,)), ((), ())), preferred_element_type=jnp.float32
    )


def across_columns(left, right):
    return lax.dot_general(
        left, right, (((1,), (1,)), ((), ())), preferred_element_type=jnp.float32
    )


def per_device(inputs, cotangent, norm_gain, gate_weight, up_weight, down_weight):
    whole_x, whole_dy = (
        lax.all_gather(inputs, ("fs", "tp"), axis=0, tiled=True),
        lax.all_gather(cotangent, ("fs", "tp"), axis=0, tiled=True),
    )
    xf = whole_x.astype(jnp.float32)
    inv = lax.rsqrt(jnp.mean(xf * xf, axis=-1, keepdims=True) + EPS)
    normed = xf * inv
    hidden_in = (normed * norm_gain).astype(jnp.bfloat16)
    gate = jnp.dot(hidden_in, gate_weight, preferred_element_type=jnp.float32)
    up = jnp.dot(hidden_in, up_weight, preferred_element_type=jnp.float32)
    sig = jax.nn.sigmoid(gate)
    act = gate * sig
    hidden = (act * up).astype(jnp.bfloat16)
    d_hidden = 0.5 * across_columns(whole_dy, down_weight)
    d_gate = (d_hidden * up * sig * (1.0 + gate * (1.0 - sig))).astype(jnp.bfloat16)
    d_up = (d_hidden * act).astype(jnp.bfloat16)
    own_rows = inputs.shape[0]
    d_in = lax.psum_scatter(
        across_columns(d_gate, gate_weight) + across_columns(d_up, up_weight),
        ("fs", "tp"),
        scatter_dimension=0,
        tiled=True,
    )
    offset = lax.axis_index(("fs", "tp")) * own_rows
    own_normed = lax.dynamic_slice_in_dim(normed, offset, own_rows, 0)
    own_inv = lax.dynamic_slice_in_dim(inv, offset, own_rows, 0)
    gain_grad = lax.psum(jnp.sum(d_in * own_normed, axis=0), ("rep", "fs", "tp"))
    scaled = d_in * norm_gain
    input_grad = (
        own_inv * (scaled - own_normed * jnp.mean(scaled * own_normed, axis=-1, keepdims=True))
    ).astype(jnp.bfloat16)
    input_grad, gain_grad = (input_grad, gain_grad)
    part_down = 0.5 * across_tokens(whole_dy, hidden)
    got_down = lax.all_to_all(
        part_down[None].astype(jnp.bfloat16), "rep", split_axis=1, concat_axis=0, tiled=True
    ).astype(jnp.float32)
    down_grad = jnp.sum(got_down, axis=0).T
    return (input_grad, gain_grad, down_grad)


def solution(mesh):
    return jax.shard_map(
        per_device,
        mesh=mesh,
        in_specs=(
            P(("rep", "fs", "tp"), None),
            P(("rep", "fs", "tp"), None),
            P(),
            P(None, ("fs", "tp")),
            P(None, ("fs", "tp")),
            P(("fs", "tp"), None),
        ),
        out_specs=(P(("rep", "fs", "tp"), None), P(), P(("fs", "tp"), "rep")),
        check_vma=False,
    )
```

profile of v0, /device:TPU:0, one launch (start us, length us, event | category | flops | bytes accessed | tf_op | source)
XLA Modules:
  0.0 166.7 jit_solution(2304956729085242355)
XLA Ops:
  7.2 0.0 copy-start
  7.2 0.0 reduce-scatter.2.cloned.1.call-start
  7.2 11.8 %all_gather.6 = bf16[128,2048]{1,0:T(8,128)(2,1)S(1)} all-gather(bf16[16,2048]{1,0:T(8,128)(2,1)} %param.6), channel_id=1, replica_groups=mesh['rep'=4,'fs'=4,'tp'=2] {'fs','tp'}, dimensions={0}, use_global_device_ids=true | all-gather | bytes 589824 | tf_op jit(solution)/shard_map/all_gather | solution.py:23
  19.0 0.2 fusion.2
  19.2 0.0 copy-done
  19.2 1.4 fusion.3
  20.6 0.0 copy-start.6
  20.7 0.0 copy-start.3
  20.7 0.6 fusion.4
  21.3 0.3 copy-done.6
  21.6 9.5 %all_gather.7 = bf16[128,2048]{1,0:T(8,128)(2,1)S(1)} all-gather(bf16[16,2048]{1,0:T(8,128)(2,1)S(1)} %copy-done.6), channel_id=1, replica_groups=mesh['rep'=4,'fs'=4,'tp'=2] {'fs','tp'}, dimensions={0}, use_global_device_ids=true | all-gather | bytes 589824 | tf_op jit(solution)/shard_map/all_gather | solution.py:24
  31.1 0.8 copy-done.1
  31.9 0.5 convolution_multiply_fusion.1
  32.4 0.5 fusion.6
  33.0 1.5 convolution_add_fusion
  34.5 0.0 reduce-scatter.2.cloned.1.call-update
  34.5 1.8 %fusion.1 = bf16[1,2048,352]{1,2,0:T(8,128)(2,1)S(1)} fusion(bf16[128,2048]{1,0:T(8,128)(2,1)} %copy-done.1, f32[128,352]{0,1:T(8,128)} %copy-done.5, f32[128,352]{0,1:T(8,128)} %copy-done.2), kind=kOutput, calls=%fused_computation.2 | convolution fusion | flops 186261504 | bytes 2326528 | tf_op jit(solution)/shard_map/dot_general | solution.py:10
  36.3 5.7 %copy.12 = bf16[1,2048,352]{2,0,1:T(2,128)(2,1)} copy(bf16[1,2048,352]{1,2,0:T(8,128)(2,1)S(1)} %fusion.1) | data formatting | bytes 2883584 | tf_op jit(solution)/shard_map/convert_element_type | solution.py:56
  42.0 0.5 broadcast.53
  42.5 34.4 %reduce = bf16[2048,352]{1,0:T(8,128)(2,1)S(1)} reduce(bf16[2048,1,352]{2,1,0:T(2,128)(2,1)} %bitcast.16, bf16[]{:T(256)} %broadcast.53), dimensions={1}, to_apply=%bitcast.7.reduce_sub_computation | reduce | bytes 2883586
  76.9 3.6 %reshape.41 = bf16[4,2,90112]{2,1,0:T(2,128)(2,1)} reshape(bf16[2048,352]{1,0:T(8,128)(2,1)S(1)} %reduce) | data formatting | bytes 2883584
  80.5 4.9 %all-to-all-start = ((bf16[4,2,90112]{2,1,0:T(2,128)(2,1)}), bf16[4,2,90112]{2,1,0:T(2,128)(2,1)S(1)}, u32[]{:S(2)}, u32[]{:S(2)}) async-start(bf16[4,2,90112]{2,1,0:T(2,128)(2,1)} %reshape.41), calls=%async_computation.1 | async-start | bytes 2883584 | tf_op jit(solution)/shard_map/all_to_all | solution.py:55
  85.3 0.1 dynamic-slice.3
  85.4 1.1 convert_multiply_fusion
  86.5 1.1 multiply_reduce_fusion
  87.6 51.7 %psum.7 = f32[2048]{0:T(1024)} all-reduce(f32[2048]{0:T(1024)S(1)} %get-tuple-element.3), channel_id=1, replica_groups=mesh['rep'=4,'fs'=4,'tp'=2] {'rep','fs','tp'}, use_global_device_ids=true, to_apply=%region_4.0 | all-reduce | flops 2048 | bytes 16384 | tf_op jit(solution)/shard_map/psum | solution.py:48
  139.4 1.7 %multiply_convert_fusion.6 = bf16[16,2048]{1,0:T(8,128)(2,1)} fusion(f32[16,2048]{1,0:T(8,128)} %reduce-scatter.2.cloned.1.call-done, f32[128,2048]{1,0:T(8,128)} %convert_multiply_fusion, s32[]{:T(128)S(6)} %select_n.4, f32[16]{0:T(128)S(1)} %broadcast_multiply_fusion, f32[2048]{0:T(1024)S(1)} %copy-done.7, f32[16]{0:T(128)S(1)} %dynamic-slice.3), kind=kLoop, calls=%fused_computation.17 | loop fusion | flops 163840 | bytes 336004 | tf_op jit(solution)/shard_map/convert_element_type | solution.py:52
  141.0 0.0 all-to-all-done
  141.1 4.0 %reshape.42 = bf16[2048,1,352]{2,1,0:T(2,128)(2,1)} reshape(bf16[4,2,90112]{2,1,0:T(2,128)(2,1)S(1)} %all-to-all-done) | data formatting | bytes 2883584
  145.0 7.0 %copy.13 = bf16[1,2048,352]{1,2,0:T(8,128)(2,1)S(1)} copy(bf16[1,2048,352]{2,0,1:T(2,128)(2,1)} %bitcast.17) | data formatting | bytes 2883584 | tf_op jit(solution)/shard_map/all_to_all | solution.py:55
  152.0 3.4 %reshape.40 = f32[4,512,352]{1,0,2:T(4,128)} reshape(bf16[1,2048,352]{1,2,0:T(8,128)(2,1)S(1)} %copy.13) | data formatting | bytes 4325376 | tf_op jit(solution)/shard_map/convert_element_type | solution.py:57
  155.5 4.4 %reduce_sum.39 = f32[512,352]{0,1:T(8,128)} reduce(f32[4,512,352]{1,0,2:T(4,128)} %reshape.40, f32[]{:T(128)} %constant.11.clone.1), dimensions={0}, to_apply=%region_5.0 | reduce | flops 540672 | bytes 3604484 | tf_op jit(solution)/shard_map/reduce_sum | solution.py:58
  (13 shorter events, 0.0 us)
Async XLA Ops:
  7.2 12.0 %copy-start = (bf16[2048,352]{0,1:T(8,128)(2,1)S(1)}, bf16[2048,352]{0,1:T(8,128)(2,1)}, u32[]{:S(2)}) copy-start(bf16[2048,352]{0,1:T(8,128)(2,1)} %param.9) | copy-start | bytes 4325380
  7.2 79.3 %reduce-scatter.2.cloned.1.call-start = ((), (), s32[]{:S(2)}) async-start(), calls=%async_computation.2 | async-start | bytes 1179648 | tf_op jit(solution)/shard_map/reduce_scatter | solution.py:39
  19.0 1.6 copy-start.4
  19.0 1.6 copy-start.7
  20.6 12.3 %copy-start.2 = (f32[128,352]{0,1:T(8,128)}, f32[128,352]{0,1:T(8,128)S(1)}, u32[]{:S(2)}) copy-start(f32[128,352]{0,1:T(8,128)S(1)} %fusion.3) | copy-start | bytes 540676
  20.6 0.9 copy-start.6
  20.7 11.2 %copy-start.3 = (bf16[352,2048]{1,0:T(8,128)(2,1)S(1)}, bf16[352,2048]{1,0:T(8,128)(2,1)}, u32[]{:S(2)}) copy-start(bf16[352,2048]{1,0:T(8,128)(2,1)} %param.11) | copy-start | bytes 4325380
  21.6 11.4 %copy-start.5 = (f32[128,352]{0,1:T(8,128)}, f32[128,352]{0,1:T(8,128)S(1)}, u32[]{:S(2)}) copy-start(f32[128,352]{0,1:T(8,128)S(1)} %fusion.4) | copy-start | bytes 540676
  31.1 0.8 copy-start.1
  80.5 60.6 %all-to-all-start = ((bf16[4,2,90112]{2,1,0:T(2,128)(2,1)}), bf16[4,2,90112]{2,1,0:T(2,128)(2,1)S(1)}, u32[]{:S(2)}, u32[]{:S(2)}) async-start(bf16[4,2,90112]{2,1,0:T(2,128)(2,1)} %reshape.41), calls=%async_computation.1 | async-start | bytes 2883584 | tf_op jit(solution)/shard_map/all_to_all | solution.py:55
Sparse Core Ops, SparseCore 0:
  34.6 36.2 reduce-scatter.1
where the time goes:
time: 167 us
  blocking collectives  73 us (44%)
  other arithmetic  42.9 us (26%)
  local copies, waits for them, and re-layouts  25.4 us (15%)
  between operations  14.2 us (9%)
  matrix products  6.35 us (4%)
  starting transfers between devices  4.91 us (3%)
    psum x1, blocking collectives, per_device(): lax.psum(jnp.sum(d_in * own_normed, axis=0), ('rep', 'fs', 'tp'))  51.7 us
    unnamed x1, other arithmetic  34.4 us
    all_gather x1, blocking collectives, per_device(): lax.all_gather(inputs, ('fs', 'tp'), axis=0, tiled=True)  11.8 us
    all_gather x1, blocking collectives, per_device(): lax.all_gather(cotangent, ('fs', 'tp'), axis=0, tiled=True)  9.52 us
    unnamed x19, local copies, waits for them, and re-layouts  9.19 us
    all_to_all x1, local copies, waits for them, and re-layouts, per_device(): lax.all_to_all(part_down[None].astype(jnp.bfloat16), 'rep', split_axis=1,...  7.01 us
    convert_element_type x1, local copies, waits for them, and re-layouts, per_device(): part_down[None].astype(jnp.bfloat16)  5.72 us
    all_to_all x1, starting transfers between devices, per_device(): lax.all_to_all(part_down[None].astype(jnp.bfloat16), 'rep', split_axis=1,...  4.87 us
  transfers between devices with their start and end apart: 2, of which 0 were waited for; matrix products, arithmetic and copies ran while one was open for 30% of the time, Pallas kernels for 0%

commit v1 on v0

--- a/solution.py
+++ b/solution.py
@@ -45,7 +45,9 @@
     offset = lax.axis_index(("fs", "tp")) * own_rows
     own_normed = lax.dynamic_slice_in_dim(normed, offset, own_rows, 0)
     own_inv = lax.dynamic_slice_in_dim(inv, offset, own_rows, 0)
-    gain_grad = lax.psum(jnp.sum(d_in * own_normed, axis=0), ("rep", "fs", "tp"))
+    gain_grad = jnp.sum(d_in * own_normed, axis=0)
+    for w in ("rep", ("fs", "tp")):
+        gain_grad = lax.psum(gain_grad, w)
     scaled = d_in * norm_gain
     input_grad = (
         own_inv * (scaled - own_normed * jnp.mean(scaled * own_normed, axis=-1, keepdims=True))

time: 167 us -> 161 us (0.964)
  the two profiles are of different devices: /device:TPU:0 before, /device:TPU:16 now
where the time goes in v1:
time: 161 us; the launch traced here: 160 us
  blocking collectives  66.3 us (41%)
  other arithmetic  42.8 us (27%)
  local copies, waits for them, and re-layouts  25.4 us (16%)
  between operations  14.2 us (9%)
  matrix products  6.35 us (4%)
  starting transfers between devices  5.24 us (3%)
    psum x2, blocking collectives, per_device(): gain_grad = lax.psum(gain_grad, w)  46.5 us
    unnamed x1, other arithmetic  34.4 us
    all_gather x1, blocking collectives, per_device(): lax.all_gather(inputs, ('fs', 'tp'), axis=0, tiled=True)  10.3 us
    all_gather x1, blocking collectives, per_device(): lax.all_gather(cotangent, ('fs', 'tp'), axis=0, tiled=True)  9.52 us
    unnamed x19, local copies, waits for them, and re-layouts  9.19 us
    all_to_all x1, local copies, waits for them, and re-layouts, per_device(): lax.all_to_all(part_down[None].astype(jnp.bfloat16), 'rep', split_axis=1,...  7.01 us
    convert_element_type x1, local copies, waits for them, and re-layouts, per_device(): part_down[None].astype(jnp.bfloat16)  5.72 us
    all_to_all x1, starting transfers between devices, per_device(): lax.all_to_all(part_down[None].astype(jnp.bfloat16), 'rep', split_axis=1,...  5.21 us
  transfers between devices with their start and end apart: 2, of which 0 were waited for; matrix products, arithmetic and copies ran while one was open for 31% of the time, Pallas kernels for 0%

profile of v1, /device:TPU:16, one launch (start us, length us, event | category | flops | bytes accessed | tf_op | source)
XLA Modules:
  0.0 160.3 jit_solution(4573061655616328672)
XLA Ops:
  7.2 0.0 copy-start
  7.2 0.0 reduce-scatter.2.cloned.1.call-start
  7.2 10.3 %all_gather.6 = bf16[128,2048]{1,0:T(8,128)(2,1)S(1)} all-gather(bf16[16,2048]{1,0:T(8,128)(2,1)} %param.6), channel_id=1, replica_groups=mesh['rep'=4,'fs'=4,'tp'=2] {'fs','tp'}, dimensions={0}, use_global_device_ids=true | all-gather | bytes 589824 | tf_op jit(solution)/shard_map/all_gather | solution.py:23
  17.5 0.2 fusion.2
  17.7 1.4 fusion.3
  19.2 0.0 copy-start.6
  19.2 0.0 copy-start.3
  19.2 0.6 fusion.4
  19.8 0.3 copy-done.6
  20.1 9.5 %all_gather.7 = bf16[128,2048]{1,0:T(8,128)(2,1)S(1)} all-gather(bf16[16,2048]{1,0:T(8,128)(2,1)S(1)} %copy-done.6), channel_id=1, replica_groups=mesh['rep'=4,'fs'=4,'tp'=2] {'fs','tp'}, dimensions={0}, use_global_device_ids=true | all-gather | bytes 589824 | tf_op jit(solution)/shard_map/all_gather | solution.py:24
  29.6 0.8 copy-done.1
  30.4 0.5 convolution_multiply_fusion.1
  30.9 0.5 fusion.6
  31.5 1.5 convolution_add_fusion
  33.0 0.0 reduce-scatter.2.cloned.1.call-update
  33.0 1.8 %fusion.1 = bf16[1,2048,352]{1,2,0:T(8,128)(2,1)S(1)} fusion(bf16[128,2048]{1,0:T(8,128)(2,1)} %copy-done.1, f32[128,352]{0,1:T(8,128)} %copy-done.5, f32[128,352]{0,1:T(8,128)} %copy-done.2), kind=kOutput, calls=%fused_computation.2 | convolution fusion | flops 186261504 | bytes 2326528 | tf_op jit(solution)/shard_map/dot_general | solution.py:10
  34.8 5.7 %copy.12 = bf16[1,2048,352]{2,0,1:T(2,128)(2,1)} copy(bf16[1,2048,352]{1,2,0:T(8,128)(2,1)S(1)} %fusion.1) | data formatting | bytes 2883584 | tf_op jit(solution)/shard_map/convert_element_type | solution.py:58
  40.5 0.5 broadcast.53
  41.0 34.4 %reduce = bf16[2048,352]{1,0:T(8,128)(2,1)S(1)} reduce(bf16[2048,1,352]{2,1,0:T(2,128)(2,1)} %bitcast.16, bf16[]{:T(256)} %broadcast.53), dimensions={1}, to_apply=%bitcast.7.reduce_sub_computation | reduce | bytes 2883586
  75.4 3.6 %reshape.41 = bf16[4,2,90112]{2,1,0:T(2,128)(2,1)} reshape(bf16[2048,352]{1,0:T(8,128)(2,1)S(1)} %reduce) | data formatting | bytes 2883584
  79.0 5.2 %all-to-all-start = ((bf16[4,2,90112]{2,1,0:T(2,128)(2,1)}), bf16[4,2,90112]{2,1,0:T(2,128)(2,1)S(1)}, u32[]{:S(2)}, u32[]{:S(2)}) async-start(bf16[4,2,90112]{2,1,0:T(2,128)(2,1)} %reshape.41), calls=%async_computation.1 | async-start | bytes 2883584 | tf_op jit(solution)/shard_map/all_to_all | solution.py:57
  84.2 0.1 dynamic-slice.3
  84.3 1.1 convert_multiply_fusion
  85.4 1.1 multiply_reduce_fusion
  86.5 33.7 %psum.14 = f32[2048]{0:T(1024)S(1)} all-reduce(f32[2048]{0:T(1024)S(1)} %get-tuple-element.3), channel_id=1, replica_groups=mesh['rep'=4,'fs'=4,'tp'=2] {'rep'}, use_global_device_ids=true, to_apply=%region_4.0 | all-reduce | flops 2048 | bytes 16384 | tf_op jit(solution)/shard_map/psum | solution.py:50
  120.2 12.8 %psum.15 = f32[2048]{0:T(1024)} all-reduce(f32[2048]{0:T(1024)S(1)} %psum.14), channel_id=1, replica_groups=mesh['rep'=4,'fs'=4,'tp'=2] {'fs','tp'}, use_global_device_ids=true, to_apply=%region_5.0 | all-reduce | flops 2048 | bytes 16384 | tf_op jit(solution)/shard_map/psum | solution.py:50
  133.0 1.7 %multiply_convert_fusion.6 = bf16[16,2048]{1,0:T(8,128)(2,1)} fusion(f32[16,2048]{1,0:T(8,128)} %reduce-scatter.2.cloned.1.call-done, f32[128,2048]{1,0:T(8,128)} %convert_multiply_fusion, s32[]{:T(128)S(6)} %select_n.4, f32[16]{0:T(128)S(1)} %broadcast_multiply_fusion, f32[2048]{0:T(1024)S(1)} %copy-done.7, f32[16]{0:T(128)S(1)} %dynamic-slice.3), kind=kLoop, calls=%fused_computation.17 | loop fusion | flops 163840 | bytes 336004 | tf_op jit(solution)/shard_map/convert_element_type | solution.py:54
  134.7 0.0 all-to-all-done
  134.7 4.0 %reshape.42 = bf16[2048,1,352]{2,1,0:T(2,128)(2,1)} reshape(bf16[4,2,90112]{2,1,0:T(2,128)(2,1)S(1)} %all-to-all-done) | data formatting | bytes 2883584
  138.6 7.0 %copy.13 = bf16[1,2048,352]{1,2,0:T(8,128)(2,1)S(1)} copy(bf16[1,2048,352]{2,0,1:T(2,128)(2,1)} %bitcast.17) | data formatting | bytes 2883584 | tf_op jit(solution)/shard_map/all_to_all | solution.py:57
  145.7 3.4 %reshape.40 = f32[4,512,352]{1,0,2:T(4,128)} reshape(bf16[1,2048,352]{1,2,0:T(8,128)(2,1)S(1)} %copy.13) | data formatting | bytes 4325376 | tf_op jit(solution)/shard_map/convert_element_type | solution.py:59
  149.1 4.4 %reduce_sum.39 = f32[512,352]{0,1:T(8,128)} reduce(f32[4,512,352]{1,0,2:T(4,128)} %reshape.40, f32[]{:T(128)} %constant.11.clone.1), dimensions={0}, to_apply=%region_6.0 | reduce | flops 540672 | bytes 3604484 | tf_op jit(solution)/shard_map/reduce_sum | solution.py:60
  (14 shorter events, 0.0 us)
Async XLA Ops:
  7.2 10.6 %copy-start = (bf16[2048,352]{0,1:T(8,128)(2,1)S(1)}, bf16[2048,352]{0,1:T(8,128)(2,1)}, u32[]{:S(2)}) copy-start(bf16[2048,352]{0,1:T(8,128)(2,1)} %param.9) | copy-start | bytes 4325380
  7.2 78.2 %reduce-scatter.2.cloned.1.call-start = ((), (), s32[]{:S(2)}) async-start(), calls=%async_computation.2 | async-start | bytes 1179648 | tf_op jit(solution)/shard_map/reduce_scatter | solution.py:39
  17.5 1.6 %copy-start.4 = (bf16[2048,352]{0,1:T(8,128)(2,1)S(1)}, bf16[2048,352]{0,1:T(8,128)(2,1)}, u32[]{:S(2)}) copy-start(bf16[2048,352]{0,1:T(8,128)(2,1)} %param.10) | copy-start | bytes 4325380
  17.5 1.6 %copy-start.7 = (f32[2048]{0:T(1024)S(1)}, f32[2048]{0:T(1024)}, u32[]{:S(2)}) copy-start(f32[2048]{0:T(1024)} %param.8) | copy-start | bytes 24580
  19.2 12.3 %copy-start.2 = (f32[128,352]{0,1:T(8,128)}, f32[128,352]{0,1:T(8,128)S(1)}, u32[]{:S(2)}) copy-start(f32[128,352]{0,1:T(8,128)S(1)} %fusion.3) | copy-start | bytes 540676
  19.2 0.9 copy-start.6
  19.2 11.2 %copy-start.3 = (bf16[352,2048]{1,0:T(8,128)(2,1)S(1)}, bf16[352,2048]{1,0:T(8,128)(2,1)}, u32[]{:S(2)}) copy-start(bf16[352,2048]{1,0:T(8,128)(2,1)} %param.11) | copy-start | bytes 4325380
  20.1 11.4 %copy-start.5 = (f32[128,352]{0,1:T(8,128)}, f32[128,352]{0,1:T(8,128)S(1)}, u32[]{:S(2)}) copy-start(f32[128,352]{0,1:T(8,128)S(1)} %fusion.4) | copy-start | bytes 540676
  29.6 0.8 copy-start.1
  79.0 55.7 %all-to-all-start = ((bf16[4,2,90112]{2,1,0:T(2,128)(2,1)}), bf16[4,2,90112]{2,1,0:T(2,128)(2,1)S(1)}, u32[]{:S(2)}, u32[]{:S(2)}) async-start(bf16[4,2,90112]{2,1,0:T(2,128)(2,1)} %reshape.41), calls=%async_computation.1 | async-start | bytes 2883584 | tf_op jit(solution)/shard_map/all_to_all | solution.py:57
Sparse Core Ops, SparseCore 0:
  33.1 36.0 reduce-scatter.1
